TPU v7x, 32 devices: a whole 2x2x4 slice. The times are simulated.
32 devices in a mesh: fs: 8 (over z, y), tp: 4 (over x, core).
Axes of the slice: x: 2, y: 2, z: 4, core: 2. Of those that a mesh axis runs over, the one named last changes fastest.
Arguments:
- inputs: bfloat16 [4096, 2048], P(('fs', 'tp')), may hold values from -6 to 6
- w_gate: float32 [2048, 5632], P('fs', 'tp'), may hold values from -0.125 to 0.125
- w_value: float32 [2048, 5632], P('fs', 'tp'), may hold values from -0.125 to 0.125
- gate_scale: float32 [5632], P('tp'), may hold values from 0.5 to 2
- value_scale: float32 [5632], P('tp'), may hold values from 0.5 to 2
- conv_gate: float32 [3, 5632], P(None, 'tp'), may hold values from -3.5 to 3.5
- conv_value: float32 [3, 5632], P(None, 'tp'), may hold values from -3.5 to 3.5
- gate_pre: bfloat16 [4096, 5632], P('fs', 'tp'), may hold values from -6 to 6
- value_pre: bfloat16 [4096, 5632], P('fs', 'tp'), may hold values from -6 to 6
- grad_out: bfloat16 [4096, 5632], P('fs', 'tp'), may hold values from -6 to 6
Outputs:
- grad_inputs: bfloat16 [4096, 2048], P(('fs', 'tp'))
- grad_w_gate: float32 [2048, 5632], P('fs', 'tp')
- grad_w_value: float32 [2048, 5632], P('fs', 'tp')
- grad_gate_scale: float32 [5632], P('tp')
- grad_value_scale: float32 [5632], P('tp')
- grad_conv_gate: float32 [3, 5632], P(None, 'tp')
- grad_conv_value: float32 [3, 5632], P(None, 'tp')
All inputs are finite; a program needn't handle non-finite values.
Results may differ from a plain program's by a relative error of at most 0.015.
Values may be sent and summed in bfloat16 or wider, within the bound.
A program may use at most 128 MiB of HBM per device.

v0:
```python
import functools

import jax
import jax.numpy as jnp
from jax import lax
from jax.experimental import pallas as pl
from jax.experimental.pallas import tpu as pltpu
from jax.sharding import PartitionSpec as P


BF = jnp.bfloat16
F32 = jnp.float32


LANES = 128


def elementwise(gs_ref, vs_ref, cg_ref, cv_ref, g_ref, v_ref, up_ref, gc_ref, vc_ref, s_ref):
    tokens = g_ref.shape[0]
    row = lax.broadcasted_iota(jnp.int32, g_ref.shape, 0)

    def down(x, k):
        return jnp.where(row >= k, pltpu.roll(x, k, 0), 0.0)

    def up(x, k):
        return jnp.where(row < tokens - k, pltpu.roll(x, tokens - k, 0), 0.0)

    def shifted(ref):
        x = ref[...].astype(F32)
        return down(x, 2), down(x, 1), x

    def conv(taps, xs):
        return taps[0:1] * xs[0] + taps[1:2] * xs[1] + taps[2:3] * xs[2]

    def back(taps, d):
        return (taps[2:3] * d + taps[1:2] * up(d, 1) + taps[0:1] * up(d, 2)).astype(BF)

    gs, vs = shifted(g_ref), shifted(v_ref)
    g = conv(cg_ref[...] * gs_ref[...], gs)
    v = conv(cv_ref[...] * vs_ref[...], vs)
    sig = 1.0 / (1.0 + jnp.exp(-g))
    base = up_ref[...].astype(F32) * sig
    d_gate = base * v * (1.0 + g * (1.0 - sig))
    d_value = base * g
    for j in range(3):
        s_ref[j : j + 1] = jnp.sum(d_gate * gs[j], axis=0, keepdims=True)
        s_ref[3 + j : 4 + j] = jnp.sum(d_value * vs[j], axis=0, keepdims=True)
    s_ref[6:8] = jnp.zeros((2, g_ref.shape[1]), F32)
    gc_ref[...] = back(cg_ref[...], d_gate)
    vc_ref[...] = back(cv_ref[...], d_value)


def cotangents(gs, vs, cg, cv, g, v, up):
    tokens, columns = g.shape
    big = pl.BlockSpec((tokens, LANES), lambda i: (0, i))

    def small(n):
        return pl.BlockSpec((n, LANES), lambda i: (0, i))

    return pl.pallas_call(
        elementwise,
        grid=(pl.cdiv(columns, LANES),),
        in_specs=[small(1), small(1), small(3), small(3), big, big, big],
        out_specs=[big, big, small(8)],
        out_shape=[jax.ShapeDtypeStruct(g.shape, BF)] * 2
        + [jax.ShapeDtypeStruct((8, columns), F32)],
        compiler_params=pltpu.CompilerParams(vmem_limit_bytes=24 * 2**20),
        cost_estimate=pl.CostEstimate(
            flops=g.size * 400, bytes_accessed=g.size * 10, transcendentals=g.size
        ),
    )(gs[None], vs[None], cg, cv, g, v, up)


def rescale(gs_ref, vs_ref, g_ref, v_ref, out_ref):
    out_ref[0] = (g_ref[...] * gs_ref[...]).astype(BF)
    out_ref[1] = (v_ref[...] * vs_ref[...]).astype(BF)


def scaled_weights(gs, vs, g, v):
    own, columns = g.shape
    parts = 4
    block = pl.BlockSpec((own // parts, columns), lambda i: (i, 0))
    scale = pl.BlockSpec((1, columns), lambda i: (0, 0))
    return pl.pallas_call(
        rescale,
        grid=(parts,),
        in_specs=[scale, scale, block, block],
        out_specs=pl.BlockSpec((2, own // parts, columns), lambda i: (0, i, 0)),
        out_shape=jax.ShapeDtypeStruct((2, own, columns), BF),
        compiler_params=pltpu.CompilerParams(vmem_limit_bytes=24 * 2**20),
        cost_estimate=pl.CostEstimate(
            flops=g.size * 100, bytes_accessed=g.size * 12, transcendentals=0
        ),
    )(gs[None], vs[None], g, v)


def tdot(a, b):
    return lax.dot_general(a, b, (((0,), (0,)), ((), ())), preferred_element_type=F32)


def ndot(a, b):
    return lax.dot_general(a, b, (((1,), (1,)), ((), ())), preferred_element_type=F32)


def make(n_fs, n_tp):
    links = n_fs // 2

    def on_device(
        inputs,
        w_gate,
        w_value,
        gate_scale,
        value_scale,
        conv_gate,
        conv_value,
        gate_pre,
        value_pre,
        grad_out,
    ):
        fs = lax.axis_index("fs")
        tp = lax.axis_index("tp")
        c, y = fs // 2, fs % 2
        rows, depth = inputs.shape
        own = w_gate.shape[0]
        half = depth // 2
        tokens, columns = gate_pre.shape

        def swap(x, axis, bit, n):
            return lax.ppermute(x, axis, [(i, i ^ bit) for i in range(n)])

        def chain(x, right, senders):
            step = 1 if right else -1
            pairs = [(2 * s + j, 2 * (s + step) + j) for s in senders for j in (0, 1)]
            return lax.ppermute(x, "fs", pairs)

        stacked = scaled_weights(gate_scale, value_scale, w_gate, w_value)
        rights, lefts = [], []
        r = l = stacked
        for s in range(links - 1):
            r = chain(r, True, range(s, links - 1))
            l = chain(l, False, range(1, links - s))
            rights.append(r)
            lefts.append(l)

        by_half = inputs.reshape(rows, links, 2, own)
        mine = lax.dynamic_index_in_dim(by_half, y, 2, keepdims=False)
        other = lax.dynamic_index_in_dim(by_half, 1 - y, 2, keepdims=False)
        mine, other = mine.reshape(rows, half), other.reshape(rows, half)
        other = swap(other, "fs", 1, n_fs)
        x = jnp.stack([mine, other])[:, None]
        bit = n_tp // 2
        while bit:
            got = swap(x, "tp", bit, n_tp)
            high = (tp // bit) % 2 == 1
            x = jnp.where(high, jnp.stack([got, x], 2), jnp.stack([x, got], 2))
            x = x.reshape(2, -1, rows, half)
            bit //= 2
        x = x.reshape(2, tokens, half)

        gate_cot, value_cot, sums = cotangents(
            gate_scale, value_scale, conv_gate, conv_value, gate_pre, value_pre, grad_out
        )
        bit = n_fs // 2
        while bit:
            sums = sums + swap(sums, "fs", bit, n_fs)
            bit //= 2

        gate_theirs = swap(gate_cot, "fs", 1, n_fs)
        value_theirs = swap(value_cot, "fs", 1, n_fs)
        pair = [(gate_cot, gate_theirs), (value_cot, value_theirs)]

        def at(blocks, i):
            return lax.dynamic_index_in_dim(
                blocks, jnp.clip(i, 0, links - 1), 0, keepdims=False
            )

        def collect(parts):
            r = l = None
            for t in range(links - 1):
                send_r = at(parts, links - 1 - t + c)
                send_l = at(parts, c - (links - 1 - t) + 0)
                if t:
                    send_r = (send_r.astype(F32) + r.astype(F32)).astype(BF)
                    send_l = (send_l.astype(F32) + l.astype(F32)).astype(BF)
                r = chain(send_r, True, range(0, t + 1))
                l = chain(send_l, False, range(links - 1 - t, links))
            total = at(parts, c).astype(F32)
            if r is not None:
                total = total + r.astype(F32) + l.astype(F32)
            return total

        grads = []
        for (cot, theirs), scale in zip(pair, (gate_scale, value_scale)):
            first = tdot(x[0], cot)
            parts = (first + tdot(x[1], theirs)).astype(BF)
            blocks = parts.reshape(links, own, columns)
            grads.append(collect(blocks) * scale)

        blocks = [stacked]
        for s in range(links - 1):
            blocks.append(jnp.where(c > s, rights[s], lefts[links - 2 - s]))
        columns_of = []
        for block in blocks:
            columns_of.append(
                [
                    (ndot(g, block[0]) + ndot(v, block[1])).astype(BF)
                    for g, v in zip(pair[0], pair[1])
                ]
            )
        part = jnp.stack([jnp.concatenate(t, 1) for t in zip(*columns_of)])
        part = part.reshape(2, n_tp, rows, half)
        bit = 1
        while bit < n_tp:
            split = part.reshape(2, -1, 2, rows, half)
            which = (tp // bit) % 2
            keep = lax.dynamic_index_in_dim(split, which, 2, keepdims=False)
            send = lax.dynamic_index_in_dim(split, 1 - which, 2, keepdims=False)
            got = swap(send, "tp", bit, n_tp)
            part = (keep.astype(F32) + got.astype(F32)).astype(BF)
            bit *= 2
        mine = part.reshape(2, rows, half)[0]
        other = swap(part.reshape(2, rows, half)[1], "fs", 1, n_fs)
        both = jnp.where(
            y == 0, jnp.stack([mine, other], 1), jnp.stack([other, mine], 1)
        ).reshape(rows, 2, links, own)
        order = (c - jnp.arange(links)) % links
        grad_inputs = jnp.take(both, order, axis=2).transpose(0, 2, 1, 3)
        return (
            grad_inputs.reshape(rows, depth),
            grads[0],
            grads[1],
            jnp.sum(conv_gate * sums[0:3], axis=0),
            jnp.sum(conv_value * sums[3:6], axis=0),
            sums[0:3] * gate_scale,
            sums[3:6] * value_scale,
        )

    return on_device


MESH = pl.DeviceIdType.MESH
SKEW = 2


def segments(links, pieces):
    table = []
    for pos in range(links - 1):
        reach = links - 1 - pos
        rows, count, last = [], 0, None
        for tick in range(pieces + SKEW * (reach - 1)):
            live = [k for k in range(reach) if 0 <= tick - SKEW * k < pieces]
            key = (live[0], len(live)) if live else None
            if key and key != last:
                rows.append((count, tick, live[0], len(live)))
            last = key
            count += len(live)
        table.append(rows)
    return table


def fused(dims, *refs):
    n_fs, n_tp = dims
    (
        inp, wg, wv, gs, vs, cg, cv, gp, vp, up,
        gi, gwg, gwv, ggs, gvs, gcg, gcv,
        wraw, pre, wbuf, cot, part, rs0, rs1, xin, xs, xb, xt,
        acc, dxb, dx1, ds1, dx2, ds2, dx3, stage, fin, sown, spair, sfrom, sgot, sput,
        load_sem, ag_sem, rs_sem, z_sem, y_sem, ysend_sem, xsend_sem, xrecv_sem,
        dsend_sem, drecv_sem, ssend_sem, srecv_sem, out_sem,
    ) = refs
    rs = (rs0, rs1)
    links = n_fs // 2
    pieces = cot.shape[0]
    own = wg.shape[0]
    rows, _ = inp.shape
    tokens = gp.shape[0]
    slots = links * pieces

    fs = lax.axis_index("fs")
    tp = lax.axis_index("tp")
    c, y = lax.div(fs, 2), lax.rem(fs, 2)
    xx, core = lax.div(tp, 2), lax.rem(tp, 2)
    y_dev = (fs + 1 - 2 * y, tp)
    x_dev = (fs, tp + 2 - 4 * xx)
    core_dev = (fs, tp + 1 - 2 * core)
    x_tp = tp + 2 - 4 * xx
    position = (c, links - 1 - c)
    follower = ((fs + 2, tp), (fs - 2, tp))

    def real(way, index):
        return index if way == 0 else links - 1 - index

    def remote(src, dst, send, recv, device):
        return pltpu.make_async_remote_copy(
            src_ref=src, dst_ref=dst, send_sem=send, recv_sem=recv,
            device_id=device, device_id_type=MESH,
        )

    def lanes(j):
        return pl.ds(pl.multiple_of(j * LANES, LANES), LANES)

    loads = [
        pltpu.make_async_copy(wg, wraw.at[0], load_sem.at[0]),
        pltpu.make_async_copy(wv, wraw.at[1], load_sem.at[1]),
        pltpu.make_async_copy(inp, xin, load_sem.at[2]),
        pltpu.make_async_copy(gp, pre.at[0], load_sem.at[3]),
        pltpu.make_async_copy(vp, pre.at[1], load_sem.at[4]),
        pltpu.make_async_copy(up, pre.at[2], load_sem.at[5]),
    ]
    for copy in loads:
        copy.start()

    barrier = pltpu.get_barrier_semaphore()
    for device in (y_dev, x_dev, core_dev):
        pl.semaphore_signal(barrier, inc=1, device_id=device, device_id_type=MESH)
    for way in (0, 1):
        @pl.when(position[way] < links - 1)
        def _():
            pl.semaphore_signal(barrier, inc=1, device_id=follower[way], device_id_type=MESH)
    inner = jnp.where((c > 0) & (c < links - 1), 5, 4)
    pl.semaphore_wait(barrier, inner)

    def ag_copy(way, o, j):
        return remote(
            wbuf.at[o, j], wbuf.at[o, j], z_sem.at[way], ag_sem.at[way, o, j], follower[way]
        )

    def rs_copy(way, src, t, j):
        return remote(
            src.at[t, j], rs[way].at[t, j], z_sem.at[way], rs_sem.at[way, t, j], follower[way]
        )

    def y_copy(j):
        return remote(
            cot.at[j, pl.ds(0, tokens)], cot.at[j, pl.ds(tokens, tokens)],
            ysend_sem.at[0], y_sem.at[j], y_dev,
        )

    loads[0].wait()
    loads[1].wait()

    def weights(j, _):
        at = lanes(j)
        wbuf[c, j, :, 0:LANES] = (wraw[0, :, at] * gs[:, at]).astype(BF)
        wbuf[c, j, :, LANES : 2 * LANES] = (wraw[1, :, at] * vs[:, at]).astype(BF)
        for way in (0, 1):
            @pl.when(position[way] < links - 1)
            def _():
                ag_copy(way, c, j).start()
        return 0

    lax.fori_loop(0, pieces, weights, 0)

    loads[2].wait()
    for o in range(links):
        for h in (0, 1):
            block = xin[:, (2 * o + h) * own : (2 * o + h + 1) * own]

            @pl.when(y == h)
            def _():
                xb[0, tp, :, o * own : (o + 1) * own] = block

            @pl.when(y != h)
            def _():
                xs[:, o * own : (o + 1) * own] = block

    xy = remote(xs, xb.at[1, tp], xsend_sem.at[0], xrecv_sem.at[0], y_dev)
    xy.start()
    xx0 = remote(xb.at[0, tp], xb.at[0, tp], xsend_sem.at[1], xrecv_sem.at[1], x_dev)
    xx0.start()
    xc0 = remote(xb.at[0, tp], xb.at[0, tp], xsend_sem.at[2], xrecv_sem.at[2], core_dev)
    xc0.start()

    for k in (3, 4, 5):
        loads[k].wait()

    row = lax.broadcasted_iota(jnp.int32, (tokens, LANES), 0)

    def down(a, k):
        return jnp.where(row >= k, pltpu.roll(a, k, 0), 0.0)

    def upward(a, k):
        return jnp.where(row < tokens - k, pltpu.roll(a, tokens - k, 0), 0.0)

    def elements(j, _):
        at = lanes(j)

        def shifted(i):
            a = pre[i, :, at].astype(F32)
            return down(a, 2), down(a, 1), a

        def conv(taps, a):
            return taps[0:1] * a[0] + taps[1:2] * a[1] + taps[2:3] * a[2]

        def back(taps, d):
            return (taps[2:3] * d + taps[1:2] * upward(d, 1) + taps[0:1] * upward(d, 2)).astype(BF)

        tg, tv = cg[:, at], cv[:, at]
        ga, va = shifted(0), shifted(1)
        g = conv(tg * gs[:, at], ga)
        v = conv(tv * vs[:, at], va)
        sig = 1.0 / (1.0 + jnp.exp(-g))
        base = pre[2, :, at].astype(F32) * sig
        d_gate = base * v * (1.0 + g * (1.0 - sig))
        d_value = base * g
        cot[j, 0:tokens, 0:LANES] = back(tg, d_gate)
        cot[j, 0:tokens, LANES : 2 * LANES] = back(tv, d_value)
        y_copy(j).start()
        for k in range(3):
            sown[k : k + 1, at] = jnp.sum(d_gate * ga[k], axis=0, keepdims=True)
            sown[3 + k : 4 + k, at] = jnp.sum(d_value * va[k], axis=0, keepdims=True)
        sown[6:8, at] = jnp.zeros((2, LANES), F32)
        return 0

    lax.fori_loop(0, pieces, elements, 0)

    sy = remote(sown, sfrom, ssend_sem.at[2], srecv_sem.at[2], y_dev)
    sy.start()

    xy.wait_recv()
    xx1 = remote(xb.at[1, tp], xb.at[1, tp], xsend_sem.at[3], xrecv_sem.at[3], x_dev)
    xx1.start()
    xc1 = remote(xb.at[1, tp], xb.at[1, tp], xsend_sem.at[4], xrecv_sem.at[4], core_dev)
    xc1.start()
    xx0.wait_recv()
    xc2 = remote(xb.at[0, x_tp], xb.at[0, x_tp], xsend_sem.at[5], xrecv_sem.at[5], core_dev)
    xc2.start()
    xx1.wait_recv()
    xc3 = remote(xb.at[1, x_tp], xb.at[1, x_tp], xsend_sem.at[6], xrecv_sem.at[6], core_dev)
    xc3.start()
    for copy in (xc0, xc1, xc2, xc3):
        copy.wait_recv()
    for q in (0, 1):
        for i in range(n_tp):
            for o in range(links):
                at = (q * n_tp + i) * rows
                xt[o, :, at : at + rows] = xb[q, i, :, o * own : (o + 1) * own].T

    def wait_y(j):
        y_copy(j).wait_recv()

    def partial(j):
        def one(o, _):
            part[o, j] = jnp.dot(xt[o], cot[j], preferred_element_type=F32).astype(BF)
            return 0

        lax.fori_loop(0, links, one, 0)

    table = segments(links, pieces)

    def decode(p, n):
        m = n - pieces * (p + 1)
        k, j = jnp.int32(0), jnp.int32(0)
        for first, tick, low, count in table[p]:
            q = lax.div(m - first, count)
            kk = low + (m - first) - q * count
            here = m >= first
            k = jnp.where(here, kk, k)
            j = jnp.where(here, tick + q - SKEW * kk, j)
        return k, j

    def relay(way, n):
        pos = position[way]

        @pl.when((pos < links - 1) & (n < pieces * (pos + 1)))
        def _():
            q = lax.div(n, pieces)
            j = n - q * pieces
            copy = ag_copy(way, real(way, pos - q), j)
            copy.wait_recv()
            copy.start()

        @pl.when((pos < links - 1) & (n >= pieces * (pos + 1)) & (n < slots))
        def _():
            k, j = decode(0, n)
            for p in range(1, links - 1):
                kp, jp = decode(p, n)
                k, j = jnp.where(pos == p, kp, k), jnp.where(pos == p, jp, j)
            t = real(way, links - 1 - k)

            @pl.when(pos == 0)
            def _():
                rs_copy(way, part, t, j).start()

            @pl.when(pos > 0)
            def _():
                rs_copy(way, part, t, j).wait_recv()
                rs[way][t, j] = (rs[way][t, j].astype(F32) + part[t, j].astype(F32)).astype(BF)
                rs_copy(way, rs[way], t, j).start()

    start = (5 * pieces) // 2

    def sum_copy(way):
        return remote(
            sput.at[way], sgot.at[way], ssend_sem.at[way], srecv_sem.at[way], follower[way]
        )

    def sums_step(way, n):
        pos = position[way]

        @pl.when((n == start + 1 + 2 * pos) & (pos < links - 1))
        def _():
            @pl.when(pos == 0)
            def _():
                sput[way] = spair[...]

            @pl.when(pos > 0)
            def _():
                sum_copy(way).wait_recv()
                sput[way] = spair[...] + sgot[way]

            sum_copy(way).start()

    dx_at = [start + 2 * p for p in range(links - 1)] + [(links - 1) * pieces + 3]
    order = [sorted(range(links), key=lambda o, a=a: (abs(o - a), o)) for a in range(links)]

    def block_at(n, shift):
        p_is = [n == at + shift for at in dx_at]
        o = jnp.int32(0)
        for a in range(links):
            for p in range(links):
                o = jnp.where(p_is[p] & (c == a), order[a][p], o)
        hit = p_is[0]
        for one in p_is[1:]:
            hit = hit | one
        return hit, o

    def core_copy(o):
        return remote(
            dxb.at[o, 1 - core], dx1.at[o], dsend_sem.at[0, o], drecv_sem.at[0, o], core_dev
        )

    def across_copy(o):
        return remote(
            ds1.at[o, 1 - xx], dx2.at[o], dsend_sem.at[1, o], drecv_sem.at[1, o], x_dev
        )

    def home_copy(o):
        return remote(
            ds2.at[o, 1], dx3.at[o], dsend_sem.at[2, o], drecv_sem.at[2, o], y_dev
        )

    first_late = len([n for n in range(slots) if pieces <= n <= start and _is_lead(table, pieces, n)])

    def dx_steps(n):
        hit, o = block_at(n, 0)

        @pl.when(hit)
        def _():
            for way in (0, 1):
                @pl.when((position[way] == links - 1) & (o != c))
                def _():
                    def one(j, _):
                        ag_copy(way, o, j).wait_recv()
                        return 0

                    lax.fori_loop(0, pieces, one, 0)

            acc[...] = ndot(cot[0], wbuf[o, 0])

            def one(j, _):
                acc[...] += ndot(cot[j], wbuf[o, j])
                return 0

            lax.fori_loop(1, pieces, one, 0)
            for q in (0, 1):
                for i in range(n_tp):
                    at = (q * n_tp + i) * rows
                    dxb[o, i % 2, i // 2, q] = acc[at : at + rows].astype(BF)
            core_copy(o).start()

        hit1, o1 = block_at(n, 1)

        @pl.when(hit1)
        def _():
            core_copy(o1).wait_recv()
            ds1[o1] = (dxb[o1, core].astype(F32) + dx1[o1].astype(F32)).astype(BF)
            across_copy(o1).start()

        hit2, o2 = block_at(n, 3)

        @pl.when(hit2)
        def _():
            across_copy(o2).wait_recv()
            ds2[o2] = (ds1[o2, xx].astype(F32) + dx2[o2].astype(F32)).astype(BF)
            home_copy(o2).start()

    def out_copy(j, k):
        dst = gwg if k == 0 else gwv
        return pltpu.make_async_copy(stage.at[j, k], dst.at[:, lanes(j)], out_sem.at[j, k])

    def final(j):
        fin[...] = part[c, j].astype(F32)
        for way in (0, 1):
            @pl.when(position[way] > 0)
            def _():
                rs_copy(way, part, c, j).wait_recv()
                fin[...] += rs[way][c, j].astype(F32)
        at = lanes(j)
        stage[j, 0] = fin[:, 0:LANES] * gs[:, at]
        stage[j, 1] = fin[:, LANES : 2 * LANES] * vs[:, at]
        for k in (0, 1):
            out_copy(j, k).start()

    wait_y(0)
    partial(0)
    last = (links - 1) * pieces + 3

    def slot(n, _):
        for way in (0, 1):
            relay(way, n)
            sums_step(way, n)

        @pl.when(n == start)
        def _():
            for late in range(first_late, pieces):
                wait_y(late)
            sy.wait_recv()
            spair[...] = sown[...] + sfrom[...]

        k, j = decode(0, n + 1)

        @pl.when((k == 0) & (n + 1 < slots))
        def _():
            @pl.when(n < start)
            def _():
                wait_y(j)

            partial(j)

        dx_steps(n)

        @pl.when(n >= last)
        def _():
            final(n - last)

        return 0

    lax.fori_loop(pieces, last + pieces, slot, 0)

    for o in range(links):
        home_copy(o).wait_recv()
        for h in (0, 1):
            at = (2 * o + h) * own

            @pl.when(y == h)
            def _():
                gi[:, at : at + own] = ds2[o, 0]

            @pl.when(y != h)
            def _():
                gi[:, at : at + own] = dx3[o]

    for way in (0, 1):
        @pl.when(position[way] == links - 1)
        def _():
            sum_copy(way).wait_recv()

        @pl.when(position[way] > 0)
        def _():
            spair[...] += sgot[way]

    total = spair[...]
    ggs[...] = jnp.sum(cg[...] * total[0:3], axis=0, keepdims=True)
    gvs[...] = jnp.sum(cv[...] * total[3:6], axis=0, keepdims=True)
    gcg[...] = total[0:3] * gs[...]
    gcv[...] = total[3:6] * vs[...]

    for j in range(pieces):
        for k in (0, 1):
            out_copy(j, k).wait()
    for copy in (xy, xx0, xc0, xx1, xc1, xc2, xc3, sy):
        copy.wait_send()
    for o in range(links):
        core_copy(o).wait_send()
        across_copy(o).wait_send()
        home_copy(o).wait_send()
    for way in (0, 1):
        @pl.when(position[way] < links - 1)
        def _():
            sum_copy(way).wait_send()
            remote(wbuf, wbuf, z_sem.at[way], ag_sem.at[way, 0, 0], follower[way]).wait_send()
    mine = cot.at[:, pl.ds(0, tokens)]
    remote(mine, mine, ysend_sem.at[0], y_sem.at[0], y_dev).wait_send()


def _is_lead(table, pieces, n):
    m = n - pieces
    k = None
    for first, tick, low, count in table[0]:
        if m >= first:
            k = low + (m - first) % count
    return k == 0


def whole_kernel(n_fs, n_tp):
    links = n_fs // 2

    def on_device(inputs, w_gate, w_value, gate_scale, value_scale, conv_gate, conv_value,
                  gate_pre, value_pre, grad_out):
        rows, depth = inputs.shape
        own, columns = w_gate.shape
        tokens = gate_pre.shape[0]
        half = depth // 2
        pieces = columns // LANES
        anywhere = pl.BlockSpec(memory_space=pl.ANY)
        vmem = pl.BlockSpec(memory_space=pltpu.VMEM)
        dma, vm = pltpu.SemaphoreType.DMA, pltpu.VMEM
        wide = 2 * LANES
        outs = pl.pallas_call(
            functools.partial(fused, (n_fs, n_tp)),
            in_specs=[anywhere] * 3 + [vmem] * 4 + [anywhere] * 3,
            out_specs=[vmem] + [anywhere] * 2 + [vmem] * 4,
            out_shape=[
                jax.ShapeDtypeStruct((rows, depth), BF),
                jax.ShapeDtypeStruct((own, columns), F32),
                jax.ShapeDtypeStruct((own, columns), F32),
                jax.ShapeDtypeStruct((1, columns), F32),
                jax.ShapeDtypeStruct((1, columns), F32),
                jax.ShapeDtypeStruct((3, columns), F32),
                jax.ShapeDtypeStruct((3, columns), F32),
            ],
            scratch_shapes=[
                vm((2, own, columns), F32),
                vm((3, tokens, columns), BF),
                vm((links, pieces, own, wide), BF),
                vm((pieces, 2 * tokens, wide), BF),
                vm((links, pieces, own, wide), BF),
                vm((links, pieces, own, wide), BF),
                vm((links, pieces, own, wide), BF),
                vm((rows, depth), BF),
                vm((rows, half), BF),
                vm((2, n_tp, rows, half), BF),
                vm((links, own, 2 * tokens), BF),
                vm((2 * tokens, own), F32),
                vm((links, 2, 2, 2, rows, own), BF),
                vm((links, 2, 2, rows, own), BF),
                vm((links, 2, 2, rows, own), BF),
                vm((links, 2, rows, own), BF),
                vm((links, 2, rows, own), BF),
                vm((links, rows, own), BF),
                vm((pieces, 2, own, LANES), F32),
                vm((own, wide), F32),
                vm((8, columns), F32),
                vm((8, columns), F32),
                vm((8, columns), F32),
                vm((2, 8, columns), F32),
                vm((2, 8, columns), F32),
                dma((6,)),
                dma((2, links, pieces)),
                dma((2, links, pieces)),
                dma((2,)),
                dma((pieces,)),
                dma((1,)),
                dma((7,)),
                dma((7,)),
                dma((3, links)),
                dma((3, links)),
                dma((3,)),
                dma((3,)),
                dma((pieces, 2)),
            ],
            compiler_params=pltpu.CompilerParams(
                collective_id=0, has_side_effects=True, vmem_limit_bytes=60 * 2**20
            ),
        )(
            inputs, w_gate, w_value, gate_scale[None], value_scale[None], conv_gate, conv_value,
            gate_pre, value_pre, grad_out,
        )
        gi, gwg, gwv, ggs, gvs, gcg, gcv = outs
        return gi, gwg, gwv, ggs[0], gvs[0], gcg, gcv

    return on_device


def solution(mesh):
    placed = (
        P(("fs", "tp"), None),
        P("fs", "tp"),
        P("fs", "tp"),
        P("tp"),
        P("tp"),
        P(None, "tp"),
        P(None, "tp"),
        P("fs", "tp"),
        P("fs", "tp"),
        P("fs", "tp"),
    )
    body = make(mesh.shape["fs"], mesh.shape["tp"])

    given = (
        P(("fs", "tp"), None),
        P("fs", "tp"),
        P("fs", "tp"),
        P("tp"),
        P("tp"),
        P(None, "tp"),
        P(None, "tp"),
    )

    def spread(one):
        return jax.shard_map(one, mesh=mesh, in_specs=placed, out_specs=given, check_vma=False)

    step = spread(body)
    general = step
    n_fs, n_tp = mesh.shape["fs"], mesh.shape["tp"]
    fast = spread(whole_kernel(n_fs, n_tp))

    def pick(*args):
        columns = args[1].shape[1] // n_tp
        if n_tp == 4 and 2 < n_fs // 2 <= 4 and columns % LANES == 0:
            return fast(*args)
        return general(*args)

    return pick
```

profile of v0, /device:TPU:16, one launch (start us, length us, event | category | flops | bytes accessed | tf_op | source)
XLA Modules:
  0.0 146.1 jit_solution(12784960381840287597)
XLA Ops:
  0.6 1.3 broadcast_in_dim.6.refs_3_
  1.9 1.3 broadcast_in_dim.7.refs_4_
  3.2 133.4 %shard_map.153 = (bf16[128,2048]{1,0:T(8,128)(2,1)}, f32[256,1408]{1,0:T(8,128)}, f32[256,1408]{1,0:T(8,128)}, f32[1,1408]{1,0:T(1,128)}, f32[1,1408]{1,0:T(1,12...) custom-call(bf16[128,2048]{1,0:T(8,128)(2,1)} %refs_0_.1, f32[256,1408]{1,0:T(8,128)} %refs_1_.1, f32[256,1408]{1,0:T(8,128)} %refs_2_.1, ...), custom_call_target="tpu_custom_call" | custom-call | tf_op jit(solution)/shard_map/pallas_call | solution.py:710
  136.6 1.3 reduce
  137.9 1.3 reduce.1
  139.2 1.9 %copy.22 = bf16[128,2048]{1,0:T(8,128)(2,1)} copy(bf16[128,2048]{1,0:T(8,128)(2,1)} %get-tuple-element.28) | data formatting | bytes 1048576
  141.1 0.0 copy-start
  141.1 2.7 %copy.23 = f32[256,1408]{1,0:T(8,128)} copy(f32[256,1408]{1,0:T(8,128)} %get-tuple-element.29) | data formatting | bytes 2883584
  143.8 0.0 copy-done
  143.8 0.0 copy-start.2
  143.8 0.0 copy-start.1
  143.8 1.1 copy.24
  144.9 0.0 copy-done.2
  144.9 0.6 copy.25
  145.5 0.0 copy-done.1
  145.5 0.6 copy.26
Async XLA Ops:
  141.1 2.7 %copy-start = (f32[256,1408]{1,0:T(8,128)S(1)}, f32[256,1408]{1,0:T(8,128)}, u32[]{:S(2)}) copy-start(f32[256,1408]{1,0:T(8,128)} %get-tuple-element.30) | copy-start | bytes 4325380
  143.8 1.1 copy-start.2
  143.8 1.7 %copy-start.1 = (f32[3,1408]{1,0:T(4,128)S(1)}, f32[3,1408]{1,0:T(4,128)}, u32[]{:S(2)}) copy-start(f32[3,1408]{1,0:T(4,128)} %get-tuple-element.34) | copy-start | bytes 50692
where the time goes:
time: 148 us; the launch traced here: 146 us
  Pallas kernels  133 us (90%)
  local copies, waits for them, and re-layouts  9.46 us (6%)
  other arithmetic  2.62 us (2%)
    pallas_call x1, Pallas kernels, on_device(): pl.pallas_call(functools.partial(fused, (n_fs, n_tp)), in_specs=[anywhere...  133 us
    unnamed x11, local copies, waits for them, and re-layouts  6.87 us

commit v1 on v0

--- a/solution.py
+++ b/solution.py
@@ -261,12 +261,12 @@
 def fused(dims, *refs):
     n_fs, n_tp = dims
     (
-        inp, wg, wv, gs, vs, cg, cv, gp, vp, up,
-        gi, gwg, gwv, ggs, gvs, gcg, gcv,
+        inp, wg, wv, gs_in, vs_in, cg_in, cv_in, gp, vp, up,
+        gi, gw, small,
         wraw, pre, wbuf, cot, part, rs0, rs1, xin, xs, xb, xt,
-        acc, dxb, dx1, ds1, dx2, ds2, dx3, stage, fin, sown, spair, sfrom, sgot, sput,
-        load_sem, ag_sem, rs_sem, z_sem, y_sem, ysend_sem, xsend_sem, xrecv_sem,
-        dsend_sem, drecv_sem, ssend_sem, srecv_sem, out_sem,
+        acc, dxb, dx1, ds1, dx2, ds2, dx3, gs1, vs1, gs, vs, cg, cv, fin, sown, spair, sfrom, sgot, sput,
+        load_sem, hop_sem, z_sem, y_sem, ysend_sem, xsend_sem, xrecv_sem,
+        dsend_sem, drecv_sem, ssend_sem, srecv_sem,
     ) = refs
     rs = (rs0, rs1)
     links = n_fs // 2
@@ -299,16 +299,23 @@
     def lanes(j):
         return pl.ds(pl.multiple_of(j * LANES, LANES), LANES)
 
-    loads = [
-        pltpu.make_async_copy(wg, wraw.at[0], load_sem.at[0]),
-        pltpu.make_async_copy(wv, wraw.at[1], load_sem.at[1]),
-        pltpu.make_async_copy(inp, xin, load_sem.at[2]),
-        pltpu.make_async_copy(gp, pre.at[0], load_sem.at[3]),
-        pltpu.make_async_copy(vp, pre.at[1], load_sem.at[4]),
-        pltpu.make_async_copy(up, pre.at[2], load_sem.at[5]),
-    ]
-    for copy in loads:
+    def load(src, dst, k):
+        copy = pltpu.make_async_copy(src, dst, load_sem.at[k])
         copy.start()
+        return copy
+
+    def loaded(ref, k):
+        pltpu.make_async_copy(ref, ref, load_sem.at[k]).wait()
+
+    head, rest = pl.ds(0, LANES), pl.ds(LANES, (pieces - 1) * LANES)
+    scales = [load(gs_in, gs1, 4), load(vs_in, vs1, 5)]
+    for at, k in ((head, 0), (rest, 1)):
+        for i, w in enumerate((wg, wv)):
+            load(w.at[:, at], wraw.at[i, :, at], k)
+    load(inp, xin, 2)
+    for i, a in enumerate((gp, vp, up)):
+        load(a, pre.at[i], 3)
+    taps = [load(cg_in, cg, 6), load(cv_in, cv, 7)]
 
     barrier = pltpu.get_barrier_semaphore()
     for device in (y_dev, x_dev, core_dev):
@@ -322,12 +329,12 @@
 
     def ag_copy(way, o, j):
         return remote(
-            wbuf.at[o, j], wbuf.at[o, j], z_sem.at[way], ag_sem.at[way, o, j], follower[way]
+            wbuf.at[o, j], wbuf.at[o, j], z_sem.at[way], hop_sem.at[way, o, j], follower[way]
         )
 
     def rs_copy(way, src, t, j):
         return remote(
-            src.at[t, j], rs[way].at[t, j], z_sem.at[way], rs_sem.at[way, t, j], follower[way]
+            src.at[t, j], rs[way].at[t, j], z_sem.at[way], hop_sem.at[way, t, j], follower[way]
         )
 
     def y_copy(j):
@@ -336,8 +343,11 @@
             ysend_sem.at[0], y_sem.at[j], y_dev,
         )
 
-    loads[0].wait()
-    loads[1].wait()
+    for copy in scales:
+        copy.wait()
+    gs[...] = gs1[...].reshape(gs.shape)
+    vs[...] = vs1[...].reshape(vs.shape)
+    loaded(wraw.at[:, :, head], 0)
 
     def weights(j, _):
         at = lanes(j)
@@ -349,30 +359,33 @@
                 ag_copy(way, c, j).start()
         return 0
 
-    lax.fori_loop(0, pieces, weights, 0)
-
-    loads[2].wait()
+    weights(0, 0)
+    loaded(wraw.at[:, :, rest], 1)
+    lax.fori_loop(1, pieces, weights, 0)
+
+    loaded(xin, 2)
     for o in range(links):
         for h in (0, 1):
             block = xin[:, (2 * o + h) * own : (2 * o + h + 1) * own]
 
             @pl.when(y == h)
             def _():
-                xb[0, tp, :, o * own : (o + 1) * own] = block
+                xb[tp, :, o * own : (o + 1) * own] = block
 
             @pl.when(y != h)
             def _():
                 xs[:, o * own : (o + 1) * own] = block
 
-    xy = remote(xs, xb.at[1, tp], xsend_sem.at[0], xrecv_sem.at[0], y_dev)
+    xy = remote(xs, xb.at[n_tp + tp], xsend_sem.at[0], xrecv_sem.at[0], y_dev)
     xy.start()
-    xx0 = remote(xb.at[0, tp], xb.at[0, tp], xsend_sem.at[1], xrecv_sem.at[1], x_dev)
+    xx0 = remote(xb.at[tp], xb.at[tp], xsend_sem.at[0], xrecv_sem.at[1], x_dev)
     xx0.start()
-    xc0 = remote(xb.at[0, tp], xb.at[0, tp], xsend_sem.at[2], xrecv_sem.at[2], core_dev)
+    xc0 = remote(xb.at[tp], xb.at[tp], xsend_sem.at[0], xrecv_sem.at[2], core_dev)
     xc0.start()
 
-    for k in (3, 4, 5):
-        loads[k].wait()
+    loaded(pre, 3)
+    for copy in taps:
+        copy.wait()
 
     row = lax.broadcasted_iota(jnp.int32, (tokens, LANES), 0)
 
@@ -418,15 +431,15 @@
     sy.start()
 
     xy.wait_recv()
-    xx1 = remote(xb.at[1, tp], xb.at[1, tp], xsend_sem.at[3], xrecv_sem.at[3], x_dev)
+    xx1 = remote(xb.at[n_tp + tp], xb.at[n_tp + tp], xsend_sem.at[0], xrecv_sem.at[3], x_dev)
     xx1.start()
-    xc1 = remote(xb.at[1, tp], xb.at[1, tp], xsend_sem.at[4], xrecv_sem.at[4], core_dev)
+    xc1 = remote(xb.at[n_tp + tp], xb.at[n_tp + tp], xsend_sem.at[0], xrecv_sem.at[4], core_dev)
     xc1.start()
     xx0.wait_recv()
-    xc2 = remote(xb.at[0, x_tp], xb.at[0, x_tp], xsend_sem.at[5], xrecv_sem.at[5], core_dev)
+    xc2 = remote(xb.at[x_tp], xb.at[x_tp], xsend_sem.at[0], xrecv_sem.at[5], core_dev)
     xc2.start()
     xx1.wait_recv()
-    xc3 = remote(xb.at[1, x_tp], xb.at[1, x_tp], xsend_sem.at[6], xrecv_sem.at[6], core_dev)
+    xc3 = remote(xb.at[n_tp + x_tp], xb.at[n_tp + x_tp], xsend_sem.at[0], xrecv_sem.at[6], core_dev)
     xc3.start()
     for copy in (xc0, xc1, xc2, xc3):
         copy.wait_recv()
@@ -434,7 +447,7 @@
         for i in range(n_tp):
             for o in range(links):
                 at = (q * n_tp + i) * rows
-                xt[o, :, at : at + rows] = xb[q, i, :, o * own : (o + 1) * own].T
+                xt[o, :, at : at + rows] = xb[q * n_tp + i, :, o * own : (o + 1) * own].T
 
     def wait_y(j):
         y_copy(j).wait_recv()
@@ -527,17 +540,17 @@
 
     def core_copy(o):
         return remote(
-            dxb.at[o, 1 - core], dx1.at[o], dsend_sem.at[0, o], drecv_sem.at[0, o], core_dev
+            dxb.at[o, 1 - core], dx1.at[o], dsend_sem.at[0], drecv_sem.at[0, o], core_dev
         )
 
     def across_copy(o):
         return remote(
-            ds1.at[o, 1 - xx], dx2.at[o], dsend_sem.at[1, o], drecv_sem.at[1, o], x_dev
+            ds1.at[o, 1 - xx], dx2.at[o], dsend_sem.at[1], drecv_sem.at[1, o], x_dev
         )
 
     def home_copy(o):
         return remote(
-            ds2.at[o, 1], dx3.at[o], dsend_sem.at[2, o], drecv_sem.at[2, o], y_dev
+            ds2.at[o, 1], dx3.at[o], dsend_sem.at[2], drecv_sem.at[2, o], y_dev
         )
 
     first_late = len([n for n in range(slots) if pieces <= n <= start and _is_lead(table, pieces, n)])
@@ -585,10 +598,6 @@
             ds2[o2] = (ds1[o2, xx].astype(F32) + dx2[o2].astype(F32)).astype(BF)
             home_copy(o2).start()
 
-    def out_copy(j, k):
-        dst = gwg if k == 0 else gwv
-        return pltpu.make_async_copy(stage.at[j, k], dst.at[:, lanes(j)], out_sem.at[j, k])
-
     def final(j):
         fin[...] = part[c, j].astype(F32)
         for way in (0, 1):
@@ -597,10 +606,37 @@
                 rs_copy(way, part, c, j).wait_recv()
                 fin[...] += rs[way][c, j].astype(F32)
         at = lanes(j)
-        stage[j, 0] = fin[:, 0:LANES] * gs[:, at]
-        stage[j, 1] = fin[:, LANES : 2 * LANES] * vs[:, at]
-        for k in (0, 1):
-            out_copy(j, k).start()
+        gw[0, :, at] = fin[:, 0:LANES] * gs[:, at]
+        gw[1, :, at] = fin[:, LANES : 2 * LANES] * vs[:, at]
+
+    def results():
+        for o in range(links):
+            home_copy(o).wait_recv()
+            for h in (0, 1):
+                at = (2 * o + h) * own
+
+                @pl.when(y == h)
+                def _():
+                    gi[:, at : at + own] = ds2[o, 0]
+
+                @pl.when(y != h)
+                def _():
+                    gi[:, at : at + own] = dx3[o]
+
+        for way in (0, 1):
+            @pl.when(position[way] == links - 1)
+            def _():
+                sum_copy(way).wait_recv()
+
+            @pl.when(position[way] > 0)
+            def _():
+                spair[...] += sgot[way]
+
+        total = spair[...]
+        small[0:3] = total[0:3] * gs[...]
+        small[3:6] = total[3:6] * vs[...]
+        small[6:7] = jnp.sum(cg[...] * total[0:3], axis=0, keepdims=True)
+        small[7:8] = jnp.sum(cv[...] * total[3:6], axis=0, keepdims=True)
 
     wait_y(0)
     partial(0)
@@ -634,52 +670,24 @@
         def _():
             final(n - last)
 
+        @pl.when(n == last + pieces - 3)
+        def _():
+            results()
+
         return 0
 
     lax.fori_loop(pieces, last + pieces, slot, 0)
 
-    for o in range(links):
-        home_copy(o).wait_recv()
-        for h in (0, 1):
-            at = (2 * o + h) * own
-
-            @pl.when(y == h)
-            def _():
-                gi[:, at : at + own] = ds2[o, 0]
-
-            @pl.when(y != h)
-            def _():
-                gi[:, at : at + own] = dx3[o]
-
-    for way in (0, 1):
-        @pl.when(position[way] == links - 1)
-        def _():
-            sum_copy(way).wait_recv()
-
-        @pl.when(position[way] > 0)
-        def _():
-            spair[...] += sgot[way]
-
-    total = spair[...]
-    ggs[...] = jnp.sum(cg[...] * total[0:3], axis=0, keepdims=True)
-    gvs[...] = jnp.sum(cv[...] * total[3:6], axis=0, keepdims=True)
-    gcg[...] = total[0:3] * gs[...]
-    gcv[...] = total[3:6] * vs[...]
-
-    for j in range(pieces):
-        for k in (0, 1):
-            out_copy(j, k).wait()
-    for copy in (xy, xx0, xc0, xx1, xc1, xc2, xc3, sy):
-        copy.wait_send()
-    for o in range(links):
-        core_copy(o).wait_send()
-        across_copy(o).wait_send()
-        home_copy(o).wait_send()
+    seven = xb.at[pl.ds(0, 7)]
+    remote(seven, seven, xsend_sem.at[0], xrecv_sem.at[0], x_dev).wait_send()
+    sy.wait_send()
+    for ref, k in ((dx1, 0), (ds1.at[:, 0], 1), (dx3, 2)):
+        remote(ref, ref, dsend_sem.at[k], drecv_sem.at[k, 0], y_dev).wait_send()
     for way in (0, 1):
         @pl.when(position[way] < links - 1)
         def _():
             sum_copy(way).wait_send()
-            remote(wbuf, wbuf, z_sem.at[way], ag_sem.at[way, 0, 0], follower[way]).wait_send()
+            remote(wbuf, wbuf, z_sem.at[way], hop_sem.at[way, 0, 0], follower[way]).wait_send()
     mine = cot.at[:, pl.ds(0, tokens)]
     remote(mine, mine, ysend_sem.at[0], y_sem.at[0], y_dev).wait_send()
 
@@ -691,6 +699,26 @@
         if m >= first:
             k = low + (m - first) % count
     return k == 0
+
+
+def deliver(gi_in, gw_in, small, *refs):
+    gi, gwg, gwv, ggs, gvs, gcg, gcv, sg, sv, tg, tv, sem = refs
+    copies = [
+        pltpu.make_async_copy(gw_in.at[0], gwg, sem.at[0]),
+        pltpu.make_async_copy(gw_in.at[1], gwv, sem.at[1]),
+        pltpu.make_async_copy(gi_in, gi, sem.at[2]),
+    ]
+    for copy in copies:
+        copy.start()
+    tg[...] = small[0:3]
+    tv[...] = small[3:6]
+    sg[...] = small[6:7].reshape(sg.shape)
+    sv[...] = small[7:8].reshape(sv.shape)
+    for k, (src, dst) in enumerate(((tg, gcg), (tv, gcv), (sg, ggs), (sv, gvs))):
+        copies.append(pltpu.make_async_copy(src, dst, sem.at[3 + k]))
+        copies[-1].start()
+    for copy in copies:
+        copy.wait()
 
 
 def whole_kernel(n_fs, n_tp):
@@ -709,16 +737,12 @@
         wide = 2 * LANES
         outs = pl.pallas_call(
             functools.partial(fused, (n_fs, n_tp)),
-            in_specs=[anywhere] * 3 + [vmem] * 4 + [anywhere] * 3,
-            out_specs=[vmem] + [anywhere] * 2 + [vmem] * 4,
+            in_specs=[anywhere] * 10,
+            out_specs=[vmem] * 3,
             out_shape=[
-                jax.ShapeDtypeStruct((rows, depth), BF),
-                jax.ShapeDtypeStruct((own, columns), F32),
-                jax.ShapeDtypeStruct((own, columns), F32),
-                jax.ShapeDtypeStruct((1, columns), F32),
-                jax.ShapeDtypeStruct((1, columns), F32),
-                jax.ShapeDtypeStruct((3, columns), F32),
-                jax.ShapeDtypeStruct((3, columns), F32),
+                vm((rows, depth), BF),
+                vm((2, own, columns), F32),
+                vm((8, columns), F32),
             ],
             scratch_shapes=[
                 vm((2, own, columns), F32),
@@ -730,7 +754,7 @@
                 vm((links, pieces, own, wide), BF),
                 vm((rows, depth), BF),
                 vm((rows, half), BF),
-                vm((2, n_tp, rows, half), BF),
+                vm((2 * n_tp, rows, half), BF),
                 vm((links, own, 2 * tokens), BF),
                 vm((2 * tokens, own), F32),
                 vm((links, 2, 2, 2, rows, own), BF),
@@ -739,36 +763,59 @@
                 vm((links, 2, rows, own), BF),
                 vm((links, 2, rows, own), BF),
                 vm((links, rows, own), BF),
-                vm((pieces, 2, own, LANES), F32),
+                vm((columns,), F32),
+                vm((columns,), F32),
+                vm((1, columns), F32),
+                vm((1, columns), F32),
+                vm((3, columns), F32),
+                vm((3, columns), F32),
                 vm((own, wide), F32),
                 vm((8, columns), F32),
                 vm((8, columns), F32),
                 vm((8, columns), F32),
                 vm((2, 8, columns), F32),
                 vm((2, 8, columns), F32),
-                dma((6,)),
-                dma((2, links, pieces)),
+                dma((8,)),
                 dma((2, links, pieces)),
                 dma((2,)),
                 dma((pieces,)),
                 dma((1,)),
+                dma((1,)),
                 dma((7,)),
-                dma((7,)),
-                dma((3, links)),
+                dma((3,)),
                 dma((3, links)),
                 dma((3,)),
                 dma((3,)),
-                dma((pieces, 2)),
             ],
             compiler_params=pltpu.CompilerParams(
-                collective_id=0, has_side_effects=True, vmem_limit_bytes=60 * 2**20
+                collective_id=0, has_side_effects=True, vmem_limit_bytes=52 * 2**20
             ),
         )(
-            inputs, w_gate, w_value, gate_scale[None], value_scale[None], conv_gate, conv_value,
+            inputs, w_gate, w_value, gate_scale, value_scale, conv_gate, conv_value,
             gate_pre, value_pre, grad_out,
         )
-        gi, gwg, gwv, ggs, gvs, gcg, gcv = outs
-        return gi, gwg, gwv, ggs[0], gvs[0], gcg, gcv
+        return pl.pallas_call(
+            deliver,
+            in_specs=[vmem] * 3,
+            out_specs=[anywhere] * 7,
+            out_shape=[
+                jax.ShapeDtypeStruct((rows, depth), BF),
+                jax.ShapeDtypeStruct((own, columns), F32),
+                jax.ShapeDtypeStruct((own, columns), F32),
+                jax.ShapeDtypeStruct((columns,), F32),
+                jax.ShapeDtypeStruct((columns,), F32),
+                jax.ShapeDtypeStruct((3, columns), F32),
+                jax.ShapeDtypeStruct((3, columns), F32),
+            ],
+            scratch_shapes=[
+                vm((columns,), F32),
+                vm((columns,), F32),
+                vm((3, columns), F32),
+                vm((3, columns), F32),
+                dma((7,)),
+            ],
+            compiler_params=pltpu.CompilerParams(vmem_limit_bytes=2 * 2**20),
+        )(*outs)
 
     return on_device
 

time: 148 us -> 134 us (0.905)
  local copies, waits for them, and re-layouts: 9.46 us -> 0 us
  other arithmetic: 2.62 us -> 0 us
  Pallas kernels: 133 us -> 131 us
    unnamed x11 -> x0, local copies, waits for them, and re-layouts: 6.87 us -> none
    pallas_call x1, Pallas kernels: 133 us -> 129 us  [on_device(): pl.pallas_call(functools.partial(fused, (n_fs, n_tp)), in_specs=[anywhere...]
    pallas_call x2 -> x0, other arithmetic: 2.62 us -> none  [on_device(): pl.pallas_call(functools.partial(fused, (n_fs, n_tp)), in_specs=[anywhere...]
    broadcast_in_dim x2 -> x0, local copies, waits for them, and re-layouts: 2.59 us -> none  [the longest x1 1.29 us: on_device(): gate_scale[None]]
    pallas_call x0 -> x1, Pallas kernels: none -> 1.81 us  [on_device(): pl.pallas_call(deliver, in_specs=[vmem] * 3, out_specs=[anywhere] * 7, ou...]
where the time goes in v1:
time: 134 us; the launch traced here: 132 us
  Pallas kernels  131 us (98%)
    pallas_call x1, Pallas kernels, on_device(): pl.pallas_call(functools.partial(fused, (n_fs, n_tp)), in_specs=[anywhere...  129 us

profile of v1, /device:TPU:16, one launch (start us, length us, event | category | flops | bytes accessed | tf_op | source)
XLA Modules:
  0.0 131.9 jit_solution(11804659037890429265)
XLA Ops:
  0.6 129.4 %shard_map.153 = (bf16[128,2048]{1,0:T(8,128)(2,1)S(1)}, f32[2,256,1408]{2,1,0:T(8,128)S(1)}, f32[8,1408]{1,0:T(8,128)S(1)}) custom-call(bf16[128,2048]{1,0:T(8,128)(2,1)} %refs_0_.1, f32[256,1408]{1,0:T(8,128)} %refs_1_.1, f32[256,1408]{1,0:T(8,128)} %refs_2_.1, f32[1408]{0:T(1024)} %refs_3_.1, f32[1408]{0:T(1024)} %refs_4_.1, f32[3,1408]{1,0:T(4,128)} %refs_5_.1, ...), custom_call_target="tpu_custom_call" | custom-call | tf_op jit(solution)/shard_map/pallas_call | solution.py:738
  130.1 1.8 %shard_map.154 = (bf16[128,2048]{1,0:T(8,128)(2,1)}, f32[256,1408]{1,0:T(8,128)}, f32[256,1408]{1,0:T(8,128)}, f32[1408]{0:T(1024)}, f32[1408]{0:T(1024)}, /*index=5*/f32[3,1408]{1,0:T(4,128)}, f32[3,1408]{1,0:T(4,128)}) custom-call(bf16[128,2048]{1,0:T(8,128)(2,1)S(1)} %get-tuple-element.10.gi_in, f32[2,256,1408]{2,1,0:T(8,128)S(1)} %get-tuple-element.11.gw_in, ...), custom_call_target="tpu_custom_call" | custom-call | tf_op jit(solution)/shard_map/pallas_call | solution.py:797

commit v2 on v1

--- a/solution.py
+++ b/solution.py
@@ -329,13 +329,30 @@
 
     def ag_copy(way, o, j):
         return remote(
-            wbuf.at[o, j], wbuf.at[o, j], z_sem.at[way], hop_sem.at[way, o, j], follower[way]
+            wbuf.at[o, j], wbuf.at[o, j], z_sem.at[way], hop_sem.at[way, o, lax.div(j, 2)], follower[way]
         )
 
     def rs_copy(way, src, t, j):
         return remote(
-            src.at[t, j], rs[way].at[t, j], z_sem.at[way], hop_sem.at[way, t, j], follower[way]
-        )
+            src.at[t, j], rs[way].at[t, j], z_sem.at[way], hop_sem.at[way, t, lax.div(j, 2)], follower[way]
+        )
+
+    def arrived(way, ref, i, j):
+        even = lax.rem(j, 2) == 0
+
+        def take(n):
+            both = ref.at[i, pl.ds(j, n)]
+            sem = hop_sem.at[way, i, lax.div(j, 2)]
+            remote(both, both, z_sem.at[way], sem, follower[way]).wait_recv()
+
+        @pl.when(even & (j + 1 < pieces))
+        def _():
+            take(2)
+
+        if pieces % 2:
+            @pl.when(j == pieces - 1)
+            def _():
+                take(1)
 
     def y_copy(j):
         return remote(
@@ -426,9 +443,6 @@
         return 0
 
     lax.fori_loop(0, pieces, elements, 0)
-
-    sy = remote(sown, sfrom, ssend_sem.at[2], srecv_sem.at[2], y_dev)
-    sy.start()
 
     xy.wait_recv()
     xx1 = remote(xb.at[n_tp + tp], xb.at[n_tp + tp], xsend_sem.at[0], xrecv_sem.at[3], x_dev)
@@ -479,9 +493,9 @@
         def _():
             q = lax.div(n, pieces)
             j = n - q * pieces
-            copy = ag_copy(way, real(way, pos - q), j)
-            copy.wait_recv()
-            copy.start()
+            o = real(way, pos - q)
+            arrived(way, wbuf, o, j)
+            ag_copy(way, o, j).start()
 
         @pl.when((pos < links - 1) & (n >= pieces * (pos + 1)) & (n < slots))
         def _():
@@ -497,32 +511,40 @@
 
             @pl.when(pos > 0)
             def _():
-                rs_copy(way, part, t, j).wait_recv()
+                arrived(way, rs[way], t, j)
                 rs[way][t, j] = (rs[way][t, j].astype(F32) + part[t, j].astype(F32)).astype(BF)
                 rs_copy(way, rs[way], t, j).start()
 
-    start = (5 * pieces) // 2
+    start = (8 * pieces) // 3
 
     def sum_copy(way):
         return remote(
             sput.at[way], sgot.at[way], ssend_sem.at[way], srecv_sem.at[way], follower[way]
         )
 
+    sy = remote(spair, sfrom, ssend_sem.at[2], srecv_sem.at[2], y_dev)
+
     def sums_step(way, n):
         pos = position[way]
 
-        @pl.when((n == start + 1 + 2 * pos) & (pos < links - 1))
+        @pl.when(n == pieces + (pieces - 1) * pos)
         def _():
             @pl.when(pos == 0)
             def _():
-                sput[way] = spair[...]
+                sput[way] = sown[...]
 
             @pl.when(pos > 0)
             def _():
                 sum_copy(way).wait_recv()
-                sput[way] = spair[...] + sgot[way]
-
-            sum_copy(way).start()
+                sput[way] = sown[...] + sgot[way]
+
+            @pl.when(pos < links - 1)
+            def _():
+                sum_copy(way).start()
+
+    def sums_pair():
+        spair[...] = sput[0] + sput[1] - sown[...]
+        sy.start()
 
     dx_at = [start + 2 * p for p in range(links - 1)] + [(links - 1) * pieces + 3]
     order = [sorted(range(links), key=lambda o, a=a: (abs(o - a), o)) for a in range(links)]
@@ -564,18 +586,23 @@
                 @pl.when((position[way] == links - 1) & (o != c))
                 def _():
                     def one(j, _):
-                        ag_copy(way, o, j).wait_recv()
+                        arrived(way, wbuf, o, j)
                         return 0
 
                     lax.fori_loop(0, pieces, one, 0)
 
+            group = next(k for k in (5, 4, 3, 2, 1) if (pieces - 1) % k == 0)
+
+            def one(i, _):
+                new = acc[...]
+                for j in range(group):
+                    at = 1 + group * i + j
+                    new = new + ndot(cot[at], wbuf[o, at])
+                acc[...] = new
+                return 0
+
             acc[...] = ndot(cot[0], wbuf[o, 0])
-
-            def one(j, _):
-                acc[...] += ndot(cot[j], wbuf[o, j])
-                return 0
-
-            lax.fori_loop(1, pieces, one, 0)
+            lax.fori_loop(0, (pieces - 1) // group, one, 0)
             for q in (0, 1):
                 for i in range(n_tp):
                     at = (q * n_tp + i) * rows
@@ -603,7 +630,7 @@
         for way in (0, 1):
             @pl.when(position[way] > 0)
             def _():
-                rs_copy(way, part, c, j).wait_recv()
+                arrived(way, rs[way], c, j)
                 fin[...] += rs[way][c, j].astype(F32)
         at = lanes(j)
         gw[0, :, at] = fin[:, 0:LANES] * gs[:, at]
@@ -623,16 +650,8 @@
                 def _():
                     gi[:, at : at + own] = dx3[o]
 
-        for way in (0, 1):
-            @pl.when(position[way] == links - 1)
-            def _():
-                sum_copy(way).wait_recv()
-
-            @pl.when(position[way] > 0)
-            def _():
-                spair[...] += sgot[way]
-
-        total = spair[...]
+        sy.wait_recv()
+        total = spair[...] + sfrom[...]
         small[0:3] = total[0:3] * gs[...]
         small[3:6] = total[3:6] * vs[...]
         small[6:7] = jnp.sum(cg[...] * total[0:3], axis=0, keepdims=True)
@@ -651,8 +670,6 @@
         def _():
             for late in range(first_late, pieces):
                 wait_y(late)
-            sy.wait_recv()
-            spair[...] = sown[...] + sfrom[...]
 
         k, j = decode(0, n + 1)
 
@@ -665,6 +682,10 @@
             partial(j)
 
         dx_steps(n)
+
+        @pl.when(n == pieces + (pieces - 1) * (links - 1))
+        def _():
+            sums_pair()
 
         @pl.when(n >= last)
         def _():
@@ -703,20 +724,24 @@
 
 def deliver(gi_in, gw_in, small, *refs):
     gi, gwg, gwv, ggs, gvs, gcg, gcv, sg, sv, tg, tv, sem = refs
-    copies = [
-        pltpu.make_async_copy(gw_in.at[0], gwg, sem.at[0]),
-        pltpu.make_async_copy(gw_in.at[1], gwv, sem.at[1]),
-        pltpu.make_async_copy(gi_in, gi, sem.at[2]),
-    ]
-    for copy in copies:
-        copy.start()
+    copies = []
+
+    def send(src, dst):
+        copies.append(pltpu.make_async_copy(src, dst, sem.at[len(copies)]))
+        copies[-1].start()
+
+    part = gwg.shape[0] // 4
+    for i in range(4):
+        at = pl.ds(i * part, part)
+        send(gw_in.at[0, at], gwg.at[at])
+        send(gw_in.at[1, at], gwv.at[at])
+    send(gi_in, gi)
     tg[...] = small[0:3]
     tv[...] = small[3:6]
     sg[...] = small[6:7].reshape(sg.shape)
     sv[...] = small[7:8].reshape(sv.shape)
-    for k, (src, dst) in enumerate(((tg, gcg), (tv, gcv), (sg, ggs), (sv, gvs))):
-        copies.append(pltpu.make_async_copy(src, dst, sem.at[3 + k]))
-        copies[-1].start()
+    for src, dst in ((tg, gcg), (tv, gcv), (sg, ggs), (sv, gvs)):
+        send(src, dst)
     for copy in copies:
         copy.wait()
 
@@ -776,7 +801,7 @@
                 vm((2, 8, columns), F32),
                 vm((2, 8, columns), F32),
                 dma((8,)),
-                dma((2, links, pieces)),
+                dma((2, links, (pieces + 1) // 2)),
                 dma((2,)),
                 dma((pieces,)),
                 dma((1,)),
@@ -812,7 +837,7 @@
                 vm((columns,), F32),
                 vm((3, columns), F32),
                 vm((3, columns), F32),
-                dma((7,)),
+                dma((13,)),
             ],
             compiler_params=pltpu.CompilerParams(vmem_limit_bytes=2 * 2**20),
         )(*outs)

time: 134 us -> 133 us (level)
  no operation moved by 1% of the time
where the time goes in v2:
time: 133 us; the launch traced here: 132 us
  Pallas kernels  131 us (98%)
    pallas_call x1, Pallas kernels, on_device(): pl.pallas_call(functools.partial(fused, (n_fs, n_tp)), in_specs=[anywhere...  129 us

profile of v2, /device:TPU:16, one launch (start us, length us, event | category | flops | bytes accessed | tf_op | source)
XLA Modules:
  0.0 131.6 jit_solution(7536984967091994289)
XLA Ops:
  0.6 129.1 %shard_map.153 = (bf16[128,2048]{1,0:T(8,128)(2,1)S(1)}, f32[2,256,1408]{2,1,0:T(8,128)S(1)}, f32[8,1408]{1,0:T(8,128)S(1)}) custom-call(bf16[128,2048]{1,0:T(8,128)(2,1)} %refs_0_.1, f32[256,1408]{1,0:T(8,128)} %refs_1_.1, f32[256,1408]{1,0:T(8,128)} %refs_2_.1, f32[1408]{0:T(1024)} %refs_3_.1, f32[1408]{0:T(1024)} %refs_4_.1, f32[3,1408]{1,0:T(4,128)} %refs_5_.1, ...), custom_call_target="tpu_custom_call" | custom-call | tf_op jit(solution)/shard_map/pallas_call | solution.py:763
  129.7 1.9 %shard_map.154 = (bf16[128,2048]{1,0:T(8,128)(2,1)}, f32[256,1408]{1,0:T(8,128)}, f32[256,1408]{1,0:T(8,128)}, f32[1408]{0:T(1024)}, f32[1408]{0:T(1024)}, /*index=5*/f32[3,1408]{1,0:T(4,128)}, f32[3,1408]{1,0:T(4,128)}) custom-call(bf16[128,2048]{1,0:T(8,128)(2,1)S(1)} %get-tuple-element.10.gi_in, f32[2,256,1408]{2,1,0:T(8,128)S(1)} %get-tuple-element.11.gw_in, ...), custom_call_target="tpu_custom_call" | custom-call | tf_op jit(solution)/shard_map/pallas_call | solution.py:822

commit v3 on v2

--- a/solution.py
+++ b/solution.py
@@ -264,7 +264,7 @@
         inp, wg, wv, gs_in, vs_in, cg_in, cv_in, gp, vp, up,
         gi, gw, small,
         wraw, pre, wbuf, cot, part, rs0, rs1, xin, xs, xb, xt,
-        acc, dxb, dx1, ds1, dx2, ds2, dx3, gs1, vs1, gs, vs, cg, cv, fin, sown, spair, sfrom, sgot, sput,
+        acc, dxb, dx1, ds1, dx2, ds2, dx3, gs1, vs1, gs, vs, cg, cv, fin, sown, sfrom, spair, sgot, sput, stot, sall,
         load_sem, hop_sem, z_sem, y_sem, ysend_sem, xsend_sem, xrecv_sem,
         dsend_sem, drecv_sem, ssend_sem, srecv_sem,
     ) = refs
@@ -435,28 +435,48 @@
         d_value = base * g
         cot[j, 0:tokens, 0:LANES] = back(tg, d_gate)
         cot[j, 0:tokens, LANES : 2 * LANES] = back(tv, d_value)
-        y_copy(j).start()
         for k in range(3):
             sown[k : k + 1, at] = jnp.sum(d_gate * ga[k], axis=0, keepdims=True)
             sown[3 + k : 4 + k, at] = jnp.sum(d_value * va[k], axis=0, keepdims=True)
         sown[6:8, at] = jnp.zeros((2, LANES), F32)
+
+        @pl.when(j < 2)
+        def _():
+            y_copy(j).start()
+
         return 0
 
+    span = (pieces + 1) // 2 * LANES
+
+    def part_of(which):
+        return pl.ds(pl.multiple_of(which * (pieces * LANES - span), LANES), span)
+
+    def pair_copy():
+        return remote(
+            sown.at[:, part_of(1 - y)], sfrom, ssend_sem.at[2], srecv_sem.at[2], y_dev
+        )
+
+    def send_y(j, _):
+        y_copy(j).start()
+        return 0
+
     lax.fori_loop(0, pieces, elements, 0)
+    pair_copy().start()
+    lax.fori_loop(2, pieces, send_y, 0)
 
     xy.wait_recv()
     xx1 = remote(xb.at[n_tp + tp], xb.at[n_tp + tp], xsend_sem.at[0], xrecv_sem.at[3], x_dev)
     xx1.start()
-    xc1 = remote(xb.at[n_tp + tp], xb.at[n_tp + tp], xsend_sem.at[0], xrecv_sem.at[4], core_dev)
+    xc1 = remote(xb.at[n_tp + tp], xb.at[n_tp + tp], xsend_sem.at[0], xrecv_sem.at[2], core_dev)
     xc1.start()
     xx0.wait_recv()
-    xc2 = remote(xb.at[x_tp], xb.at[x_tp], xsend_sem.at[0], xrecv_sem.at[5], core_dev)
+    xc2 = remote(xb.at[x_tp], xb.at[x_tp], xsend_sem.at[0], xrecv_sem.at[2], core_dev)
     xc2.start()
     xx1.wait_recv()
-    xc3 = remote(xb.at[n_tp + x_tp], xb.at[n_tp + x_tp], xsend_sem.at[0], xrecv_sem.at[6], core_dev)
+    xc3 = remote(xb.at[n_tp + x_tp], xb.at[n_tp + x_tp], xsend_sem.at[0], xrecv_sem.at[2], core_dev)
     xc3.start()
-    for copy in (xc0, xc1, xc2, xc3):
-        copy.wait_recv()
+    four = xb.at[pl.ds(0, 4)]
+    remote(four, four, xsend_sem.at[0], xrecv_sem.at[2], core_dev).wait_recv()
     for q in (0, 1):
         for i in range(n_tp):
             for o in range(links):
@@ -522,7 +542,7 @@
             sput.at[way], sgot.at[way], ssend_sem.at[way], srecv_sem.at[way], follower[way]
         )
 
-    sy = remote(spair, sfrom, ssend_sem.at[2], srecv_sem.at[2], y_dev)
+    total_copy = remote(stot, sall, ssend_sem.at[3], srecv_sem.at[3], y_dev)
 
     def sums_step(way, n):
         pos = position[way]
@@ -531,20 +551,20 @@
         def _():
             @pl.when(pos == 0)
             def _():
-                sput[way] = sown[...]
+                sput[way] = spair[...]
 
             @pl.when(pos > 0)
             def _():
                 sum_copy(way).wait_recv()
-                sput[way] = sown[...] + sgot[way]
+                sput[way] = spair[...] + sgot[way]
 
             @pl.when(pos < links - 1)
             def _():
                 sum_copy(way).start()
 
-    def sums_pair():
-        spair[...] = sput[0] + sput[1] - sown[...]
-        sy.start()
+    def sums_total():
+        stot[...] = sput[0] + sput[1] - spair[...]
+        total_copy.start()
 
     dx_at = [start + 2 * p for p in range(links - 1)] + [(links - 1) * pieces + 3]
     order = [sorted(range(links), key=lambda o, a=a: (abs(o - a), o)) for a in range(links)]
@@ -650,8 +670,11 @@
                 def _():
                     gi[:, at : at + own] = dx3[o]
 
-        sy.wait_recv()
-        total = spair[...] + sfrom[...]
+        total_copy.wait_recv()
+        pair_copy().wait_send()
+        for h in (0, 1):
+            sown[:, part_of(h)] = jnp.where(y == h, stot[...], sall[...])
+        total = sown[...]
         small[0:3] = total[0:3] * gs[...]
         small[3:6] = total[3:6] * vs[...]
         small[6:7] = jnp.sum(cg[...] * total[0:3], axis=0, keepdims=True)
@@ -659,6 +682,8 @@
 
     wait_y(0)
     partial(0)
+    pair_copy().wait_recv()
+    spair[...] = sown[:, part_of(y)] + sfrom[...]
     last = (links - 1) * pieces + 3
 
     def slot(n, _):
@@ -685,7 +710,7 @@
 
         @pl.when(n == pieces + (pieces - 1) * (links - 1))
         def _():
-            sums_pair()
+            sums_total()
 
         @pl.when(n >= last)
         def _():
@@ -701,7 +726,7 @@
 
     seven = xb.at[pl.ds(0, 7)]
     remote(seven, seven, xsend_sem.at[0], xrecv_sem.at[0], x_dev).wait_send()
-    sy.wait_send()
+    total_copy.wait_send()
     for ref, k in ((dx1, 0), (ds1.at[:, 0], 1), (dx3, 2)):
         remote(ref, ref, dsend_sem.at[k], drecv_sem.at[k, 0], y_dev).wait_send()
     for way in (0, 1):
@@ -730,11 +755,8 @@
         copies.append(pltpu.make_async_copy(src, dst, sem.at[len(copies)]))
         copies[-1].start()
 
-    part = gwg.shape[0] // 4
-    for i in range(4):
-        at = pl.ds(i * part, part)
-        send(gw_in.at[0, at], gwg.at[at])
-        send(gw_in.at[1, at], gwv.at[at])
+    send(gw_in.at[0], gwg)
+    send(gw_in.at[1], gwv)
     send(gi_in, gi)
     tg[...] = small[0:3]
     tv[...] = small[3:6]
@@ -760,6 +782,7 @@
         vmem = pl.BlockSpec(memory_space=pltpu.VMEM)
         dma, vm = pltpu.SemaphoreType.DMA, pltpu.VMEM
         wide = 2 * LANES
+        span = (pieces + 1) // 2 * LANES
         outs = pl.pallas_call(
             functools.partial(fused, (n_fs, n_tp)),
             in_specs=[anywhere] * 10,
@@ -796,21 +819,23 @@
                 vm((3, columns), F32),
                 vm((own, wide), F32),
                 vm((8, columns), F32),
-                vm((8, columns), F32),
-                vm((8, columns), F32),
-                vm((2, 8, columns), F32),
-                vm((2, 8, columns), F32),
+                vm((8, span), F32),
+                vm((8, span), F32),
+                vm((2, 8, span), F32),
+                vm((2, 8, span), F32),
+                vm((8, span), F32),
+                vm((8, span), F32),
                 dma((8,)),
                 dma((2, links, (pieces + 1) // 2)),
                 dma((2,)),
                 dma((pieces,)),
                 dma((1,)),
                 dma((1,)),
-                dma((7,)),
+                dma((4,)),
                 dma((3,)),
                 dma((3, links)),
-                dma((3,)),
-                dma((3,)),
+                dma((4,)),
+                dma((4,)),
             ],
             compiler_params=pltpu.CompilerParams(
                 collective_id=0, has_side_effects=True, vmem_limit_bytes=52 * 2**20
@@ -837,7 +862,7 @@
                 vm((columns,), F32),
                 vm((3, columns), F32),
                 vm((3, columns), F32),
-                dma((13,)),
+                dma((7,)),
             ],
             compiler_params=pltpu.CompilerParams(vmem_limit_bytes=2 * 2**20),
         )(*outs)

time: 133 us -> 133 us (level)
  no operation moved by 1% of the time
where the time goes in v3:
time: 133 us; the launch traced here: 131 us
  Pallas kernels  130 us (98%)
    pallas_call x1, Pallas kernels, on_device(): pl.pallas_call(functools.partial(fused, (n_fs, n_tp)), in_specs=[anywhere...  129 us

profile of v3, /device:TPU:16, one launch (start us, length us, event | category | flops | bytes accessed | tf_op | source)
XLA Modules:
  0.0 131.1 jit_solution(12896489101479583156)
XLA Ops:
  0.6 128.6 %shard_map.153 = (bf16[128,2048]{1,0:T(8,128)(2,1)S(1)}, f32[2,256,1408]{2,1,0:T(8,128)S(1)}, f32[8,1408]{1,0:T(8,128)S(1)}) custom-call(bf16[128,2048]{1,0:T(8,128)(2,1)} %refs_0_.1, f32[256,1408]{1,0:T(8,128)} %refs_1_.1, f32[256,1408]{1,0:T(8,128)} %refs_2_.1, f32[1408]{0:T(1024)} %refs_3_.1, f32[1408]{0:T(1024)} %refs_4_.1, f32[3,1408]{1,0:T(4,128)} %refs_5_.1, ...), custom_call_target="tpu_custom_call" | custom-call | tf_op jit(solution)/shard_map/pallas_call | solution.py:786
  129.3 1.8 %shard_map.154 = (bf16[128,2048]{1,0:T(8,128)(2,1)}, f32[256,1408]{1,0:T(8,128)}, f32[256,1408]{1,0:T(8,128)}, f32[1408]{0:T(1024)}, f32[1408]{0:T(1024)}, /*index=5*/f32[3,1408]{1,0:T(4,128)}, f32[3,1408]{1,0:T(4,128)}) custom-call(bf16[128,2048]{1,0:T(8,128)(2,1)S(1)} %get-tuple-element.10.gi_in, f32[2,256,1408]{2,1,0:T(8,128)S(1)} %get-tuple-element.11.gw_in, ...), custom_call_target="tpu_custom_call" | custom-call | tf_op jit(solution)/shard_map/pallas_call | solution.py:847

commit v4 on v3

--- a/solution.py
+++ b/solution.py
@@ -239,7 +239,7 @@
 
 
 MESH = pl.DeviceIdType.MESH
-SKEW = 2
+SKEW = 4
 
 
 def segments(links, pieces):
@@ -258,13 +258,19 @@
     return table
 
 
+def shares(pieces):
+    body = pieces - 3
+    relays = [(i, min(4, body - i)) for i in range(0, body, 4)] + [(body, 2), (pieces - 1, 1)]
+    return relays, [(0, pieces - 5), (pieces - 5, 4), (pieces - 1, 1)]
+
+
 def fused(dims, *refs):
     n_fs, n_tp = dims
     (
         inp, wg, wv, gs_in, vs_in, cg_in, cv_in, gp, vp, up,
         gi, gw, small,
         wraw, pre, wbuf, cot, part, rs0, rs1, xin, xs, xb, xt,
-        acc, dxb, dx1, ds1, dx2, ds2, dx3, gs1, vs1, gs, vs, cg, cv, fin, sown, sfrom, spair, sgot, sput, stot, sall,
+        acc, dxb, dx1, ds1, dx2, ds2, dx3, gs1, vs1, gs, vs, tap, sown, sfrom, spair, sgot, sput, stot, sall,
         load_sem, hop_sem, z_sem, y_sem, ysend_sem, xsend_sem, xrecv_sem,
         dsend_sem, drecv_sem, ssend_sem, srecv_sem,
     ) = refs
@@ -315,7 +321,9 @@
     load(inp, xin, 2)
     for i, a in enumerate((gp, vp, up)):
         load(a, pre.at[i], 3)
-    taps = [load(cg_in, cg, 6), load(cv_in, cv, 7)]
+    load(cg_in, tap.at[0], 6)
+    load(cv_in, tap.at[1], 6)
+    cg, cv = tap.at[0], tap.at[1]
 
     barrier = pltpu.get_barrier_semaphore()
     for device in (y_dev, x_dev, core_dev):
@@ -324,35 +332,41 @@
         @pl.when(position[way] < links - 1)
         def _():
             pl.semaphore_signal(barrier, inc=1, device_id=follower[way], device_id_type=MESH)
-    inner = jnp.where((c > 0) & (c < links - 1), 5, 4)
-    pl.semaphore_wait(barrier, inner)
+    relays, ends = shares(pieces)
+
+    def index_in(groups, j):
+        g = jnp.int32(0)
+        for first, _ in groups[1:]:
+            g = g + jnp.where(j >= first, 1, 0)
+        return g
+
+    def ag_sem(way, o, j):
+        row = o if way == 0 else o - 1
+        return hop_sem.at[way, row * len(relays) + index_in(relays, j)]
+
+    def rs_sem(way, t, j, there):
+        row = t - 1 if way == 0 else t
+        relay_at = row * len(relays) + index_in(relays, j)
+        end_at = (links - 1) * len(relays) + index_in(ends, j)
+        return hop_sem.at[way, jnp.where(t == there, end_at, relay_at)]
 
     def ag_copy(way, o, j):
         return remote(
-            wbuf.at[o, j], wbuf.at[o, j], z_sem.at[way], hop_sem.at[way, o, lax.div(j, 2)], follower[way]
+            wbuf.at[o, j], wbuf.at[o, j], z_sem.at[way], ag_sem(way, o, j), follower[way]
         )
 
     def rs_copy(way, src, t, j):
+        there = c + 1 - 2 * way
         return remote(
-            src.at[t, j], rs[way].at[t, j], z_sem.at[way], hop_sem.at[way, t, lax.div(j, 2)], follower[way]
-        )
-
-    def arrived(way, ref, i, j):
-        even = lax.rem(j, 2) == 0
-
-        def take(n):
-            both = ref.at[i, pl.ds(j, n)]
-            sem = hop_sem.at[way, i, lax.div(j, 2)]
-            remote(both, both, z_sem.at[way], sem, follower[way]).wait_recv()
-
-        @pl.when(even & (j + 1 < pieces))
-        def _():
-            take(2)
-
-        if pieces % 2:
-            @pl.when(j == pieces - 1)
-            def _():
-                take(1)
+            src.at[t, j], rs[way].at[t, j], z_sem.at[way], rs_sem(way, t, j, there), follower[way]
+        )
+
+    def arrived(way, ref, i, j, sem, groups=relays):
+        for first, count in groups:
+            @pl.when(j == first)
+            def _():
+                some = ref.at[i, pl.ds(first, count)]
+                remote(some, some, z_sem.at[way], sem, follower[way]).wait_recv()
 
     def y_copy(j):
         return remote(
@@ -366,17 +380,27 @@
     vs[...] = vs1[...].reshape(vs.shape)
     loaded(wraw.at[:, :, head], 0)
 
-    def weights(j, _):
+    def scaled(j):
         at = lanes(j)
         wbuf[c, j, :, 0:LANES] = (wraw[0, :, at] * gs[:, at]).astype(BF)
         wbuf[c, j, :, LANES : 2 * LANES] = (wraw[1, :, at] * vs[:, at]).astype(BF)
+
+    def send_own(j):
         for way in (0, 1):
             @pl.when(position[way] < links - 1)
             def _():
                 ag_copy(way, c, j).start()
+
+    scaled(0)
+    inner = jnp.where((c > 0) & (c < links - 1), 5, 4)
+    pl.semaphore_wait(barrier, inner)
+
+    def weights(j, _):
+        scaled(j)
+        send_own(j)
         return 0
 
-    weights(0, 0)
+    send_own(0)
     loaded(wraw.at[:, :, rest], 1)
     lax.fori_loop(1, pieces, weights, 0)
 
@@ -401,8 +425,7 @@
     xc0.start()
 
     loaded(pre, 3)
-    for copy in taps:
-        copy.wait()
+    loaded(tap, 6)
 
     row = lax.broadcasted_iota(jnp.int32, (tokens, LANES), 0)
 
@@ -514,7 +537,7 @@
             q = lax.div(n, pieces)
             j = n - q * pieces
             o = real(way, pos - q)
-            arrived(way, wbuf, o, j)
+            arrived(way, wbuf, o, j, ag_sem(way, o, j))
             ag_copy(way, o, j).start()
 
         @pl.when((pos < links - 1) & (n >= pieces * (pos + 1)) & (n < slots))
@@ -531,7 +554,7 @@
 
             @pl.when(pos > 0)
             def _():
-                arrived(way, rs[way], t, j)
+                arrived(way, rs[way], t, j, rs_sem(way, t, j, c))
                 rs[way][t, j] = (rs[way][t, j].astype(F32) + part[t, j].astype(F32)).astype(BF)
                 rs_copy(way, rs[way], t, j).start()
 
@@ -606,7 +629,7 @@
                 @pl.when((position[way] == links - 1) & (o != c))
                 def _():
                     def one(j, _):
-                        arrived(way, wbuf, o, j)
+                        arrived(way, wbuf, o, j, ag_sem(way, o, j))
                         return 0
 
                     lax.fori_loop(0, pieces, one, 0)
@@ -646,15 +669,22 @@
             home_copy(o2).start()
 
     def final(j):
-        fin[...] = part[c, j].astype(F32)
         for way in (0, 1):
             @pl.when(position[way] > 0)
             def _():
-                arrived(way, rs[way], c, j)
-                fin[...] += rs[way][c, j].astype(F32)
+                arrived(way, rs[way], c, j, rs_sem(way, c, j, c), ends)
         at = lanes(j)
-        gw[0, :, at] = fin[:, 0:LANES] * gs[:, at]
-        gw[1, :, at] = fin[:, LANES : 2 * LANES] * vs[:, at]
+
+        def close(ways):
+            total = part[c, j].astype(F32)
+            for way in ways:
+                total = total + rs[way][c, j].astype(F32)
+            gw[0, :, at] = total[:, 0:LANES] * gs[:, at]
+            gw[1, :, at] = total[:, LANES : 2 * LANES] * vs[:, at]
+
+        pl.when((c > 0) & (c < links - 1))(lambda: close((0, 1)))
+        pl.when(c == links - 1)(lambda: close((0,)))
+        pl.when(c == 0)(lambda: close((1,)))
 
     def results():
         for o in range(links):
@@ -684,7 +714,7 @@
     partial(0)
     pair_copy().wait_recv()
     spair[...] = sown[:, part_of(y)] + sfrom[...]
-    last = (links - 1) * pieces + 3
+    last = slots - 3
 
     def slot(n, _):
         for way in (0, 1):
@@ -712,13 +742,13 @@
         def _():
             sums_total()
 
+        @pl.when(n == last + pieces - 5)
+        def _():
+            results()
+
         @pl.when(n >= last)
         def _():
             final(n - last)
-
-        @pl.when(n == last + pieces - 3)
-        def _():
-            results()
 
         return 0
 
@@ -733,7 +763,7 @@
         @pl.when(position[way] < links - 1)
         def _():
             sum_copy(way).wait_send()
-            remote(wbuf, wbuf, z_sem.at[way], hop_sem.at[way, 0, 0], follower[way]).wait_send()
+            remote(wbuf, wbuf, z_sem.at[way], hop_sem.at[way, 0], follower[way]).wait_send()
     mine = cot.at[:, pl.ds(0, tokens)]
     remote(mine, mine, ysend_sem.at[0], y_sem.at[0], y_dev).wait_send()
 
@@ -815,9 +845,7 @@
                 vm((columns,), F32),
                 vm((1, columns), F32),
                 vm((1, columns), F32),
-                vm((3, columns), F32),
-                vm((3, columns), F32),
-                vm((own, wide), F32),
+                vm((2, 3, columns), F32),
                 vm((8, columns), F32),
                 vm((8, span), F32),
                 vm((8, span), F32),
@@ -825,8 +853,8 @@
                 vm((2, 8, span), F32),
                 vm((8, span), F32),
                 vm((8, span), F32),
-                dma((8,)),
-                dma((2, links, (pieces + 1) // 2)),
+                dma((7,)),
+                dma((2, (links - 1) * len(shares(pieces)[0]) + len(shares(pieces)[1]))),
                 dma((2,)),
                 dma((pieces,)),
                 dma((1,)),
@@ -905,7 +933,7 @@
 
     def pick(*args):
         columns = args[1].shape[1] // n_tp
-        if n_tp == 4 and 2 < n_fs // 2 <= 4 and columns % LANES == 0:
+        if n_tp == 4 and 2 < n_fs // 2 <= 4 and columns % LANES == 0 and columns >= 8 * LANES:
             return fast(*args)
         return general(*args)
 

time: 133 us -> 133 us (level)
  no operation moved by 1% of the time
where the time goes in v4:
time: 133 us; the launch traced here: 131 us
  Pallas kernels  130 us (98%)
    pallas_call x1, Pallas kernels, on_device(): pl.pallas_call(functools.partial(fused, (n_fs, n_tp)), in_specs=[anywhere...  128 us

profile of v4, /device:TPU:16, one launch (start us, length us, event | category | flops | bytes accessed | tf_op | source)
XLA Modules:
  0.0 130.9 jit_solution(5744624975576219729)
XLA Ops:
  0.6 128.4 %shard_map.153 = (bf16[128,2048]{1,0:T(8,128)(2,1)S(1)}, f32[2,256,1408]{2,1,0:T(8,128)S(1)}, f32[8,1408]{1,0:T(8,128)S(1)}) custom-call(bf16[128,2048]{1,0:T(8,128)(2,1)} %refs_0_.1, f32[256,1408]{1,0:T(8,128)} %refs_1_.1, f32[256,1408]{1,0:T(8,128)} %refs_2_.1, f32[1408]{0:T(1024)} %refs_3_.1, f32[1408]{0:T(1024)} %refs_4_.1, f32[3,1408]{1,0:T(4,128)} %refs_5_.1, ...), custom_call_target="tpu_custom_call" | custom-call | tf_op jit(solution)/shard_map/pallas_call | solution.py:816
  129.1 1.8 %shard_map.154 = (bf16[128,2048]{1,0:T(8,128)(2,1)}, f32[256,1408]{1,0:T(8,128)}, f32[256,1408]{1,0:T(8,128)}, f32[1408]{0:T(1024)}, f32[1408]{0:T(1024)}, /*index=5*/f32[3,1408]{1,0:T(4,128)}, f32[3,1408]{1,0:T(4,128)}) custom-call(bf16[128,2048]{1,0:T(8,128)(2,1)S(1)} %get-tuple-element.10.gi_in, f32[2,256,1408]{2,1,0:T(8,128)S(1)} %get-tuple-element.11.gw_in, ...), custom_call_target="tpu_custom_call" | custom-call | tf_op jit(solution)/shard_map/pallas_call | solution.py:875

commit v5 on v4

--- a/solution.py
+++ b/solution.py
@@ -461,7 +461,6 @@
         for k in range(3):
             sown[k : k + 1, at] = jnp.sum(d_gate * ga[k], axis=0, keepdims=True)
             sown[3 + k : 4 + k, at] = jnp.sum(d_value * va[k], axis=0, keepdims=True)
-        sown[6:8, at] = jnp.zeros((2, LANES), F32)
 
         @pl.when(j < 2)
         def _():
@@ -846,13 +845,13 @@
                 vm((1, columns), F32),
                 vm((1, columns), F32),
                 vm((2, 3, columns), F32),
-                vm((8, columns), F32),
-                vm((8, span), F32),
-                vm((8, span), F32),
-                vm((2, 8, span), F32),
-                vm((2, 8, span), F32),
-                vm((8, span), F32),
-                vm((8, span), F32),
+                vm((6, columns), F32),
+                vm((6, span), F32),
+                vm((6, span), F32),
+                vm((2, 6, span), F32),
+                vm((2, 6, span), F32),
+                vm((6, span), F32),
+                vm((6, span), F32),
                 dma((7,)),
                 dma((2, (links - 1) * len(shares(pieces)[0]) + len(shares(pieces)[1]))),
                 dma((2,)),

time: 133 us -> 133 us (level)
  no operation moved by 1% of the time
where the time goes in v5:
time: 133 us; the launch traced here: 131 us
  Pallas kernels  130 us (98%)
    pallas_call x1, Pallas kernels, on_device(): pl.pallas_call(functools.partial(fused, (n_fs, n_tp)), in_specs=[anywhere...  128 us

profile of v5, /device:TPU:16, one launch (start us, length us, event | category | flops | bytes accessed | tf_op | source)
XLA Modules:
  0.0 130.9 jit_solution(6913736279284359160)
XLA Ops:
  0.6 128.4 %shard_map.153 = (bf16[128,2048]{1,0:T(8,128)(2,1)S(1)}, f32[2,256,1408]{2,1,0:T(8,128)S(1)}, f32[8,1408]{1,0:T(8,128)S(1)}) custom-call(bf16[128,2048]{1,0:T(8,128)(2,1)} %refs_0_.1, f32[256,1408]{1,0:T(8,128)} %refs_1_.1, f32[256,1408]{1,0:T(8,128)} %refs_2_.1, f32[1408]{0:T(1024)} %refs_3_.1, f32[1408]{0:T(1024)} %refs_4_.1, f32[3,1408]{1,0:T(4,128)} %refs_5_.1, ...), custom_call_target="tpu_custom_call" | custom-call | tf_op jit(solution)/shard_map/pallas_call | solution.py:815
  129.1 1.8 %shard_map.154 = (bf16[128,2048]{1,0:T(8,128)(2,1)}, f32[256,1408]{1,0:T(8,128)}, f32[256,1408]{1,0:T(8,128)}, f32[1408]{0:T(1024)}, f32[1408]{0:T(1024)}, /*index=5*/f32[3,1408]{1,0:T(4,128)}, f32[3,1408]{1,0:T(4,128)}) custom-call(bf16[128,2048]{1,0:T(8,128)(2,1)S(1)} %get-tuple-element.10.gi_in, f32[2,256,1408]{2,1,0:T(8,128)S(1)} %get-tuple-element.11.gw_in, ...), custom_call_target="tpu_custom_call" | custom-call | tf_op jit(solution)/shard_map/pallas_call | solution.py:874
